TPU v7x, 32 devices: a whole 2x2x4 slice. The times are simulated.
32 devices in a mesh: ep: 4 (over y, x), tp: 8 (over z, core).
Axes of the slice: x: 2, y: 2, z: 4, core: 2. Of those that a mesh axis runs over, the one named last changes fastest.
Arguments:
- queries: bfloat16 [2048, 16, 128], P('ep', 'tp'), may hold values from -125 to 125
- keys: bfloat16 [2048, 16, 128], P('ep', 'tp'), may hold values from -9 to 9
- values: bfloat16 [2048, 16, 128], P('ep', 'tp'), may hold values from -6 to 6
- mixing: float32 [16], P('tp'), may hold values from 0.3 to 0.8
- head_gain: float32 [128], replicated, may hold values from 0.1 to 1.9
- out_weight: bfloat16 [16, 128, 2048], P('tp'), may hold values from -0.125 to 0.125
- tokens_b: bfloat16 [4096, 2048], P(('ep', 'tp')), may hold values from -6 to 6
- norm_gain: float32 [2048], replicated, may hold values from 0.1 to 1.9
- expert_ids: int32 [4096, 2], P(('ep', 'tp')), may hold values from 0 to 3, all different within a row; in each aligned block of 128 rows (0 to 127, 128 to 255, ...) at most 96 rows name the same one
- group_gate: float32 [4096], P(('ep', 'tp')), may hold values from 0.2 to 1
- expert_gate: float32 [4096, 2], P(('ep', 'tp')), may hold values from 0.1 to 0.9
- gate_weight: bfloat16 [4, 2048, 1024], P('ep', None, 'tp'), may hold values from -0.125 to 0.125
- up_weight: bfloat16 [4, 2048, 1024], P('ep', None, 'tp'), may hold values from -0.125 to 0.125
- down_weight: bfloat16 [4, 2048, 1024], P('ep', None, 'tp'), may hold values from -0.1875 to 0.1875
Outputs:
- mixed: bfloat16 [2048, 2048], P(('ep', 'tp'))
- routed: bfloat16 [4096, 2048], P(('ep', 'tp'))
Inputs may be any that keep to these rules, and one draw needn't show every extreme that they name: `expert_ids`: within each aligned block of 128 rows, no expert is named by more than 96 rows, and some block has an expert named by exactly 96 rows.
All inputs are finite; a program needn't handle non-finite values.
Results may differ from a plain program's by a relative error of at most 0.019.
Values may be sent and summed in bfloat16 or wider, within the bound.
A program may use at most 192 MiB of HBM per device.

v0:
```python
import math
import jax
import jax.numpy as jnp
from jax import lax
from jax.sharding import PartitionSpec as P

HEAD = 64


def attend_heads(queries, keys, values, mixing, head_gain):
    shard_rows = queries.shape[0]
    head_count = queries.shape[1]
    value_width = values.shape[2]
    query_start = lax.axis_index("ep") * shard_rows
    score_scale = 1.0 / math.sqrt(HEAD)
    query_pos = query_start + lax.iota(jnp.int32, shard_rows)

    def update(running, key_block, value_block, block_start):
        key_pos = block_start + lax.iota(jnp.int32, shard_rows)
        allowed = key_pos[None, :] <= query_pos[:, None]
        fresh = []
        for map_index in range(2):
            maximum, row_sum, numerator = running[3 * map_index : 3 * map_index + 3]
            offset = map_index * HEAD
            scores = (
                jnp.einsum(
                    "qhd,khd->hqk",
                    queries[:, :, offset : offset + HEAD],
                    key_block[:, :, offset : offset + HEAD],
                    preferred_element_type=jnp.float32,
                )
                * score_scale
            )
            scores = jnp.where(allowed[None], scores, -1e30)
            newmax = jnp.maximum(maximum, jnp.max(scores, axis=2))
            shrink = jnp.exp(maximum - newmax)
            weights = jnp.exp(scores - newmax[:, :, None])
            row_sum = row_sum * shrink + jnp.sum(weights, axis=2)
            numerator = numerator * shrink[:, :, None] + jnp.einsum(
                "hqk,khe->hqe",
                weights.astype(jnp.bfloat16),
                value_block,
                preferred_element_type=jnp.float32,
            )
            fresh += [newmax, row_sum, numerator]
        return tuple(fresh)

    floor_max = jnp.full((head_count, shard_rows), -1e30, jnp.float32)
    zero_sum = jnp.zeros((head_count, shard_rows), jnp.float32)
    zero_acc = jnp.zeros((head_count, shard_rows, value_width), jnp.float32)
    start_state = (floor_max, zero_sum, zero_acc, floor_max, zero_sum, zero_acc)
    running = start_state
    key_piece = lax.all_gather(keys, "ep", axis=0, tiled=True)
    value_piece = lax.all_gather(values, "ep", axis=0, tiled=True)
    blocks = key_piece.shape[0] // shard_rows
    key_blocks = key_piece.reshape(blocks, shard_rows, head_count, key_piece.shape[2])
    value_blocks = value_piece.reshape(blocks, shard_rows, head_count, value_width)

    def visit_block(state, inputs):
        key_block, value_block, block_index = inputs
        block_start = block_index * shard_rows
        state = lax.cond(
            block_start <= query_start + shard_rows - 1,
            lambda state_in: update(state_in, key_block, value_block, block_start),
            lambda state_in: state_in,
            state,
        )
        return (state, None)

    running, unused = lax.scan(
        visit_block, running, (key_blocks, value_blocks, lax.iota(jnp.int32, blocks))
    )
    state = running
    diff = state[2] / state[1][:, :, None] - mixing[:, None, None] * state[5] / state[4][:, :, None]
    normed = diff * lax.rsqrt(jnp.mean(diff * diff, axis=2, keepdims=True) + 1e-05) * head_gain
    return normed.astype(jnp.bfloat16)


def mixer_half(queries, keys, values, mixing, head_gain, out_weight):
    attended = attend_heads(queries, keys, values, mixing, head_gain)
    return lax.psum_scatter(
        jnp.einsum("hqe,hed->qd", attended, out_weight, preferred_element_type=jnp.float32).astype(
            jnp.bfloat16
        ),
        "tp",
        scatter_dimension=0,
        tiled=True,
    )


def expert_half(
    tokens_b, norm_gain, expert_ids, group_gate, expert_gate, gate_weight, up_weight, down_weight
):
    local_rows = tokens_b.shape[0]
    width = tokens_b.shape[1]
    top_count = expert_ids.shape[1]
    ep_count = lax.axis_size("ep")
    local_count = gate_weight.shape[0]
    expert_total = ep_count * local_count
    capacity = 3 * local_rows * top_count // (2 * expert_total)
    tokens_f = tokens_b.astype(jnp.float32)
    normed = (
        tokens_f
        * lax.rsqrt(jnp.mean(tokens_f * tokens_f, axis=1, keepdims=True) + 1e-06)
        * norm_gain
    ).astype(jnp.bfloat16)
    flat_ids = expert_ids.reshape(-1)
    one_hot = (flat_ids[:, None] == lax.iota(jnp.int32, expert_total)[None, :]).astype(jnp.int32)
    slot_rank = jnp.sum((jnp.cumsum(one_hot, axis=0) - one_hot) * one_hot, axis=1)
    slot_index = flat_ids * capacity + slot_rank
    owners = jnp.full((expert_total * capacity,), local_rows, jnp.int32)
    owners = owners.at[slot_index].set(lax.iota(jnp.int32, local_rows * top_count) // top_count)
    padded = jnp.concatenate([normed, jnp.zeros((1, width), jnp.bfloat16)], axis=0)
    outgoing = padded[owners].reshape(ep_count, local_count * capacity, width)
    incoming = lax.all_to_all(outgoing, "ep", split_axis=0, concat_axis=0, tiled=True)
    expert_rows = jnp.transpose(
        incoming.reshape(ep_count, local_count, capacity, width), (1, 0, 2, 3)
    )
    expert_rows = expert_rows.reshape(local_count, ep_count * capacity, width)
    piece_gate = lax.all_gather(gate_weight, "tp", axis=2, tiled=True)
    piece_up = lax.all_gather(up_weight, "tp", axis=2, tiled=True)
    piece_down = lax.all_gather(down_weight, "tp", axis=2, tiled=True)
    gate_part = jnp.einsum(
        "jrd,jdf->jrf", expert_rows, piece_gate, preferred_element_type=jnp.float32
    )
    up_part = jnp.einsum("jrd,jdf->jrf", expert_rows, piece_up, preferred_element_type=jnp.float32)
    hidden = (jax.nn.silu(gate_part) * up_part).astype(jnp.bfloat16)
    expert_out = jnp.einsum(
        "jrf,jdf->jrd", hidden, piece_down, preferred_element_type=jnp.float32
    ).astype(jnp.bfloat16)
    outbound = jnp.transpose(
        expert_out.reshape(local_count, ep_count, capacity, width), (1, 0, 2, 3)
    )
    outbound = outbound.reshape(ep_count, local_count * capacity, width)
    returned = lax.all_to_all(outbound, "ep", split_axis=0, concat_axis=0, tiled=True).reshape(
        expert_total * capacity, width
    )
    picked = returned[slot_index].reshape(local_rows, top_count, width).astype(jnp.float32)
    route_weight = group_gate[:, None] * expert_gate
    return jnp.sum(route_weight[:, :, None] * picked, axis=1).astype(jnp.bfloat16)


def per_device(
    queries,
    keys,
    values,
    mixing,
    head_gain,
    out_weight,
    tokens_b,
    norm_gain,
    expert_ids,
    group_gate,
    expert_gate,
    gate_weight,
    up_weight,
    down_weight,
):
    mixed = mixer_half(queries, keys, values, mixing, head_gain, out_weight)
    routed = expert_half(
        tokens_b,
        norm_gain,
        expert_ids,
        group_gate,
        expert_gate,
        gate_weight,
        up_weight,
        down_weight,
    )
    return (mixed, routed)


def solution(mesh):
    placed = (
        P("ep", "tp", None),
        P("ep", "tp", None),
        P("ep", "tp", None),
        P("tp"),
        P(),
        P("tp", None, None),
        P(("ep", "tp"), None),
        P(),
        P(("ep", "tp"), None),
        P(("ep", "tp")),
        P(("ep", "tp"), None),
        P("ep", None, "tp"),
        P("ep", None, "tp"),
        P("ep", None, "tp"),
    )
    return jax.shard_map(
        per_device,
        mesh=mesh,
        in_specs=placed,
        out_specs=(P(("ep", "tp"), None), P(("ep", "tp"), None)),
        check_vma=False,
    )
```

profile of v0, /device:TPU:0, one launch (start us, length us, event | category | flops | bytes accessed | tf_op | source)
XLA Modules:
  0.0 260.2 jit_solution(6079203360803837472)
XLA Ops:
  7.3 1.8 copy.24
  9.1 1.7 copy.25
  13.4 1.2 reduce-window.6
  15.3 1.4 scatter_custom_fusion
  17.0 1.0 fusion.33
  17.9 21.8 %all-gather.6.cloned.1.call-done = bf16[2048,2,128]{2,0,1:T(8,128)(2,1)} async-done(((bf16[512,2,128]{2,0,1:T(8,128)(2,1)}), bf16[2048,2,128]{2,0,1:T(8,128)(2,1)}) %all-gather.6.cloned.1.call-update) | async-done | bytes 1048592 | tf_op jit(solution)/shard_map/all_gather | solution.py:53
  39.7 2.3 copy.26
  42.0 26.1 %all-gather.8.cloned.1.call-done = bf16[2048,2,128]{2,0,1:T(8,128)(2,1)} async-done(((bf16[512,2,128]{2,0,1:T(8,128)(2,1)}), bf16[2048,2,128]{2,0,1:T(8,128)(2,1)}) %all-gather.8.cloned.1.call-update) | async-done | bytes 1048592 | tf_op jit(solution)/shard_map/all_gather | solution.py:54
  68.1 1.3 copy.28
  69.5 9.8 %while.23 = (s32[]{:T(128)}, f32[2,512]{1,0:T(2,128)S(1)}, f32[2,512]{1,0:T(2,128)S(1)}, f32[2,512,128]{2,1,0:T(8,128)S(1)}, f32[2,512]{1,0:T(2,128)S(1)}, /*ind...) while((s32[]{:T(128)}, f32[2,512]{1,0:T(2,128)S(1)}, ...), condition=%wide.region_7.8_spmd.clone, body=%wide.region_0.7_spmd.clone.sunk | while | flops 410784768 | bytes 17183128 | solution.py:70
  70.8 4.6 %conditional.3 = ((f32[2,512]{1,0:T(2,128)S(1)}, f32[2,512]{1,0:T(2,128)S(1)}, f32[2,512,128]{2,1,0:T(8,128)S(1)}, f32[2,512]{1,0:T(2,128)S(1)}, f32[2,512]{1,0:T(2,128)S(1)}, /*index=5*/f32[2,512,128]{2,1,0:T(8,128)S(1)})) conditional(s32[]{:T(128)} %convert_element_type.87, (f32[2,512]{1,0:T(2,128)S(1)}, f32[2,512]{1,0:T(2,128)S(1)}, ...), branch_computations={%region_1.1_spmd, %region_2.6_spmd} | conditional | flops 410784768 | bytes 17180748 | solution.py:62
  70.8 1.0 dynamic-slice_bitcast_fusion
  79.9 2.1 bitcast_convert_fusion
  82.2 2.5 gather_fusion
  84.6 36.1 %all_to_all.10 = bf16[4,96,2048]{2,1,0:T(8,128)(2,1)} all-to-all(bf16[4,96,2048]{2,1,0:T(8,128)(2,1)S(1)} %bitcast.62), channel_id=1, replica_groups=mesh['ep'=4,'tp'=8] {'ep'}, dimensions={0} | all-to-all | bytes 3145728 | tf_op jit(solution)/shard_map/all_to_all | solution.py:115
  120.7 5.7 %fusion.24 = f32[384,1024]{1,0:T(8,128)} fusion(bf16[384,2048]{1,0:T(8,128)(2,1)} %bitcast.63, bf16[1,2048,1024]{2,1,0:T(8,128)(2,1)} %all-gather.10.cloned.1.call-done), kind=kOutput, calls=%fused_computation.38 | convolution fusion | flops 1610612736 | bytes 7340032 | tf_op jit(solution)/shard_map/jrd,jdf->jrf/dot_general | solution.py:123
  126.4 38.6 %all-gather.12.cloned.1.call-done = bf16[1,2048,1024]{2,1,0:T(8,128)(2,1)} async-done(((bf16[1,2048,128]{2,1,0:T(8,128)(2,1)}), bf16[1,2048,1024]{2,1,0:T(8,128)(2,1)}) %all-gather.12.cloned.1.call-update) | async-done | bytes 4194320 | tf_op jit(solution)/shard_map/all_gather | solution.py:121
  165.0 47.5 %all-gather.14.cloned.1.call-done = bf16[1,2048,1024]{2,1,0:T(8,128)(2,1)} async-done(((bf16[1,2048,128]{2,1,0:T(8,128)(2,1)}), bf16[1,2048,1024]{2,1,0:T(8,128)(2,1)}) %all-gather.14.cloned.1.call-update) | async-done | bytes 4194320 | tf_op jit(solution)/shard_map/all_gather | solution.py:122
  212.5 8.6 %fusion.26 = bf16[384,2048]{1,0:T(8,128)(2,1)} fusion(bf16[1,2048,1024]{2,1,0:T(8,128)(2,1)} %all-gather.14.cloned.1.call-done, f32[384,1024]{1,0:T(8,128)} %fusion.24, bf16[384,2048]{1,0:T(8,128)(2,1)S(1)} %bitcast.64, bf16[1,2048,1024]{2,1,0:T(8,128)(2,1)} %all-gather.12.cloned.1.call-done), kind=kOutput, calls=%fused_computation.41 | convolution fusion | flops 3224371200 | bytes 13107200 | tf_op jit(solution)/shard_map/jrf,jdf->jrd/dot_general | solution.py:128
  221.1 3.8 %all-to-all-start.1 = ((bf16[4,96,2048]{2,1,0:T(8,128)(2,1)}), bf16[4,96,2048]{2,1,0:T(8,128)(2,1)S(1)}, u32[]{:S(2)}, u32[]{:S(2)}) async-start(bf16[4,96,2048]{2,1,0:T(8,128)(2,1)} %bitcast.65), calls=%async_computation.2 | async-start | bytes 3145728 | tf_op jit(solution)/shard_map/all_to_all | solution.py:135
  225.0 19.7 %all-to-all-done.1 = bf16[4,96,2048]{2,1,0:T(8,128)(2,1)S(1)} async-done(((bf16[4,96,2048]{2,1,0:T(8,128)(2,1)}), bf16[4,96,2048]{2,1,0:T(8,128)(2,1)S(1)}, u32[]{:S(2)}, u32[]{:S(2)}) %all-to-all-start.1) | async-done | bytes 1572896 | tf_op jit(solution)/shard_map/all_to_all | solution.py:135
  244.7 2.3 gather_fusion.1
  247.1 2.4 reshape.163
  249.4 3.9 %multiply_reduce_fusion = bf16[128,2048]{1,0:T(8,128)(2,1)} fusion(f32[128,2,2048]{2,1,0:T(2,128)S(1)} %reshape.163, f32[128,2]{1,0:T(8,128)S(1)} %copy.29), kind=kLoop, calls=%fused_computation.42 | loop fusion | flops 786432 | bytes 2622464 | tf_op jit(solution)/shard_map/reduce_sum | solution.py:140
  (95 shorter events, 10.3 us)
Async XLA Ops:
  7.2 72.7 %copy-start = (bf16[2,128,2048]{2,1,0:T(8,128)(2,1)S(1)}, bf16[2,128,2048]{2,1,0:T(8,128)(2,1)}, u32[]{:S(2)}) copy-start(bf16[2,128,2048]{2,1,0:T(8,128)(2,1)} %param.23) | copy-start | bytes 3145732
  7.2 5.6 %copy-start.6 = (s32[128,2]{0,1:T(2,128)S(1)}, s32[128,2]{0,1:T(2,128)}, u32[]{:S(2)}) copy-start(s32[128,2]{0,1:T(2,128)} %param.26) | copy-start | bytes 3076
  7.2 6.0 %copy-start.4 = (bf16[512,2,128]{2,1,0:T(2,128)(2,1)S(1)}, bf16[512,2,128]{2,1,0:T(2,128)(2,1)}, u32[]{:S(2)}) copy-start(bf16[512,2,128]{2,1,0:T(2,128)(2,1)} %param.18) | copy-start | bytes 786436
  7.2 9.5 %copy-start.1 = (bf16[128,2048]{1,0:T(8,128)(2,1)S(1)}, bf16[128,2048]{1,0:T(8,128)(2,1)}, u32[]{:S(2)}) copy-start(bf16[128,2048]{1,0:T(8,128)(2,1)} %param.24) | copy-start | bytes 1572868
  7.2 32.5 %all-gather.6.cloned.1.call-start = ((), (), s32[]{:S(2)}) async-start(), calls=%async_computation.3 | async-start | bytes 1310720 | tf_op jit(solution)/shard_map/all_gather | solution.py:53
  9.1 7.9 %copy-start.5 = (f32[2048]{0:T(1024)S(1)}, f32[2048]{0:T(1024)}, u32[]{:S(2)}) copy-start(f32[2048]{0:T(1024)} %param.25) | copy-start | bytes 24580
  9.1 59.0 %all-gather.8.cloned.1.call-start = ((), (), s32[]{:S(2)}) async-start(), calls=%async_computation.4 | async-start | bytes 1310720 | tf_op jit(solution)/shard_map/all_gather | solution.py:54
  10.8 109.8 %all-gather.10.cloned.1.call-start = ((), (), s32[]{:S(2)}) async-start(), calls=%async_computation.6 | async-start | bytes 4718592 | tf_op jit(solution)/shard_map/all_gather | solution.py:120
  11.6 153.4 %all-gather.12.cloned.1.call-start = ((), (), s32[]{:S(2)}) async-start(), calls=%async_computation.7 | async-start | bytes 4718592 | tf_op jit(solution)/shard_map/all_gather | solution.py:121
  12.2 200.3 %all-gather.14.cloned.1.call-start = ((), (), s32[]{:S(2)}) async-start(), calls=%async_computation.8 | async-start | bytes 4718592 | tf_op jit(solution)/shard_map/all_gather | solution.py:122
  12.7 240.6 %reduce-scatter.2.cloned.1.call-start = ((), (), s32[]{:S(2)}) async-start(), calls=%async_computation.5 | async-start | bytes 2359296 | tf_op jit(solution)/shard_map/reduce_scatter | solution.py:81
  69.5 9.9 %copy-start.8 = (f32[2]{0:T(128)S(1)}, f32[2]{0:T(128)}, u32[]{:S(2)}) copy-start(f32[2]{0:T(128)} %param.21) | copy-start | bytes 28
  69.5 10.4 %copy-start.9 = (f32[128]{0:T(128)S(1)}, f32[128]{0:T(128)}, u32[]{:S(2)}) copy-start(f32[128]{0:T(128)} %param.22) | copy-start | bytes 1540
  79.9 2.2 copy-start.2
  120.7 91.8 %copy-start.3 = (bf16[4,96,2048]{2,1,0:T(8,128)(2,1)S(1)}, bf16[4,96,2048]{2,1,0:T(8,128)(2,1)}, u32[]{:S(2)}) copy-start(bf16[4,96,2048]{2,1,0:T(8,128)(2,1)} %all_to_all.10) | copy-start | bytes 4718596
  221.1 3.8 %copy-start.7 = (f32[128,2]{0,1:T(2,128)S(1)}, f32[128,2]{0,1:T(2,128)}, u32[]{:S(2)}) copy-start(f32[128,2]{0,1:T(2,128)} %param.28) | copy-start | bytes 3076
  221.1 3.8 %copy-start.10 = (f32[128]{0:T(128)S(1)}, f32[128]{0:T(128)}, u32[]{:S(2)}) copy-start(f32[128]{0:T(128)} %param.27) | copy-start | bytes 1540
  221.1 23.6 %all-to-all-start.1 = ((bf16[4,96,2048]{2,1,0:T(8,128)(2,1)}), bf16[4,96,2048]{2,1,0:T(8,128)(2,1)S(1)}, u32[]{:S(2)}, u32[]{:S(2)}) async-start(bf16[4,96,2048]{2,1,0:T(8,128)(2,1)} %bitcast.65), calls=%async_computation.2 | async-start | bytes 3145728 | tf_op jit(solution)/shard_map/all_to_all | solution.py:135
Sparse Core Ops, SparseCore 0:
  10.4 29.2 all-gather.5
  41.5 26.4 all-gather.7
  69.7 47.8 all-gather.9
  119.0 45.9 all-gather.11
  166.4 45.9 all-gather.13
  215.2 34.1 reduce-scatter.1
where the time goes:
time: 261 us; the launch traced here: 260 us
  waiting for transfers between devices  155 us (59%)
  blocking collectives  36.1 us (14%)
  local copies, waits for them, and re-layouts  20.4 us (8%)
  matrix products  19.2 us (7%)
  between operations  14.4 us (6%)
  other arithmetic  7.89 us (3%)
  starting transfers between devices  4.02 us (2%)
  loops' own time  2.93 us (1%)
    all_gather x1, waiting for transfers between devices, expert_half(): piece_down = lax.all_gather(down_weight, 'tp', axis=2, tiled=True)  47.5 us
    all_gather x1, waiting for transfers between devices, expert_half(): piece_up = lax.all_gather(up_weight, 'tp', axis=2, tiled=True)  38.6 us
    all_to_all x1, blocking collectives, expert_half(): lax.all_to_all(outgoing, 'ep', split_axis=0, concat_axis=0, tiled=True)  36.1 us
    all_gather x1, waiting for transfers between devices, attend_heads(): value_piece = lax.all_gather(values, 'ep', axis=0, tiled=True)  26.1 us
    all_gather x1, waiting for transfers between devices, attend_heads(): key_piece = lax.all_gather(keys, 'ep', axis=0, tiled=True)  21.8 us
    all_to_all x1, waiting for transfers between devices, expert_half(): lax.all_to_all(outbound, 'ep', split_axis=0, concat_axis=0, tiled=True)  19.7 us
    dot_general x1, matrix products, expert_half(): jnp.einsum('jrf,jdf->jrd', hidden, piece_down, preferred_element_type=jnp...  8.63 us
    unnamed x28, local copies, waits for them, and re-layouts  7.42 us
  transfers between devices with their start and end apart: 7, of which 5 were waited for; matrix products, arithmetic and copies ran while one was open for 18% of the time, Pallas kernels for 0%

commit v1 on v0

--- a/solution.py
+++ b/solution.py
@@ -50,7 +50,12 @@
     zero_acc = jnp.zeros((head_count, shard_rows, value_width), jnp.float32)
     start_state = (floor_max, zero_sum, zero_acc, floor_max, zero_sum, zero_acc)
     running = start_state
-    key_piece = lax.all_gather(keys, "ep", axis=0, tiled=True)
+    ring = [keys]
+    for hop in range(3):
+        ring.append(lax.ppermute(ring[-1], "ep", [(dev, (dev + 1) % 4) for dev in range(4)]))
+    key_piece = jnp.roll(
+        jnp.concatenate(ring[::-1], axis=0), (lax.axis_index("ep") + 1) * ring[0].shape[0], axis=0
+    )
     value_piece = lax.all_gather(values, "ep", axis=0, tiled=True)
     blocks = key_piece.shape[0] // shard_rows
     key_blocks = key_piece.reshape(blocks, shard_rows, head_count, key_piece.shape[2])

time: 261 us -> 239 us (0.916)
  waiting for transfers between devices: 155 us -> 135 us
  starting transfers between devices: 4.02 us -> 7.78 us
  blocking collectives: 36.1 us -> 33 us
    ppermute x0 -> x3, waiting for transfers between devices: none -> 26.6 us  [attend_heads(): lax.ppermute(ring[-1], 'ep', [(dev, (dev + 1) % 4) for dev in range(4)])]
    all_gather x1, waiting for transfers between devices: 26.1 us -> 0.01 us  [attend_heads(): value_piece = lax.all_gather(values, 'ep', axis=0, tiled=True)]
    all_gather x1 -> x0, waiting for transfers between devices: 21.8 us -> none  [attend_heads(): key_piece = lax.all_gather(keys, 'ep', axis=0, tiled=True)]
    all_gather x1, waiting for transfers between devices: 38.6 us -> 47.5 us  [expert_half(): piece_up = lax.all_gather(up_weight, 'tp', axis=2, tiled=True)]
    all_gather x1, waiting for transfers between devices: 47.5 us -> 39.4 us  [expert_half(): piece_down = lax.all_gather(down_weight, 'tp', axis=2, tiled=True)]
    ppermute x0 -> x3, starting transfers between devices: none -> 3.81 us  [attend_heads(): lax.ppermute(ring[-1], 'ep', [(dev, (dev + 1) % 4) for dev in range(4)])]
    all_to_all x1, blocking collectives: 36.1 us -> 33 us  [expert_half(): lax.all_to_all(outgoing, 'ep', split_axis=0, concat_axis=0, tiled=True)]
    unnamed x28 -> x37, local copies, waits for them, and re-layouts: 7.42 us -> 5.08 us
  transfers between devices with their start and end apart: 7 -> 9, of which waited for: 5 -> 6; matrix products, arithmetic and copies ran while one was open for 18% -> 18% of each run, Pallas kernels for 0% -> 0%
where the time goes in v1:
time: 239 us; the launch traced here: 238 us
  waiting for transfers between devices  135 us (56%)
  blocking collectives  33 us (14%)
  matrix products  19.2 us (8%)
  local copies, waits for them, and re-layouts  18.2 us (8%)
  between operations  14.1 us (6%)
  other arithmetic  7.89 us (3%)
  starting transfers between devices  7.78 us (3%)
  loops' own time  2.91 us (1%)
    all_gather x1, waiting for transfers between devices, expert_half(): piece_up = lax.all_gather(up_weight, 'tp', axis=2, tiled=True)  47.5 us
    all_gather x1, waiting for transfers between devices, expert_half(): piece_down = lax.all_gather(down_weight, 'tp', axis=2, tiled=True)  39.4 us
    all_to_all x1, blocking collectives, expert_half(): lax.all_to_all(outgoing, 'ep', split_axis=0, concat_axis=0, tiled=True)  33 us
    ppermute x3, waiting for transfers between devices, attend_heads(): lax.ppermute(ring[-1], 'ep', [(dev, (dev + 1) % 4) for dev in range(4)])  26.6 us
    all_to_all x1, waiting for transfers between devices, expert_half(): lax.all_to_all(outbound, 'ep', split_axis=0, concat_axis=0, tiled=True)  19.7 us
    dot_general x1, matrix products, expert_half(): jnp.einsum('jrf,jdf->jrd', hidden, piece_down, preferred_element_type=jnp...  8.63 us
    dot_general x1, matrix products, expert_half(): jnp.einsum('jrd,jdf->jrf', expert_rows, piece_gate, preferred_element_typ...  5.74 us
    unnamed x37, local copies, waits for them, and re-layouts  5.08 us
  transfers between devices with their start and end apart: 9, of which 6 were waited for; matrix products, arithmetic and copies ran while one was open for 18% of the time, Pallas kernels for 0%

profile of v1, /device:TPU:0, one launch (start us, length us, event | category | flops | bytes accessed | tf_op | source)
XLA Modules:
  0.0 238.1 jit_solution(17905905904219754620)
XLA Ops:
  7.3 1.8 copy.27
  11.3 3.0 %collective-permute-start = (bf16[512,2,128]{2,0,1:T(8,128)(2,1)S(1)}, bf16[512,2,128]{2,0,1:T(8,128)(2,1)S(1)}, u32[]{:S(2)}, u32[]{:S(2)}) collective-permute-start(bf16[512,2,128]{2,0,1:T(8,128)(2,1)S(1)} %copy.24), channel_id=1, source_target_pairs={{0,8},{8,16},{16,24},{24,0},{1,9},{9,17},{17,25},{25,1},{2,10},{10... | collective-permute-start | bytes 786440 | tf_op jit(solution)/shard_map/ppermute | solution.py:55
  14.8 1.0 fusion.33
  15.9 1.2 reduce-window.6
  17.5 4.0 %collective-permute-done = bf16[512,2,128]{2,0,1:T(8,128)(2,1)S(1)} collective-permute-done((bf16[512,2,128]{2,0,1:T(8,128)(2,1)S(1)}, bf16[512,2,128]{2,0,1:T(8,128)(2,1)S(1)}, u32[]{:S(2)}, u32[]{:S(2)}) %collective-permute-start) | collective-permute-done | bytes 262176 | tf_op jit(solution)/shard_map/ppermute | solution.py:55
  22.6 10.0 %collective-permute-done.1 = bf16[512,2,128]{2,0,1:T(8,128)(2,1)S(1)} collective-permute-done((bf16[512,2,128]{2,0,1:T(8,128)(2,1)S(1)}, bf16[512,2,128]{2,0,1:T(8,128)(2,1)S(1)}, u32[]{:S(2)}, u32[]{:S(2)}) %collective-permute-start.1) | collective-permute-done | bytes 262176 | tf_op jit(solution)/shard_map/ppermute | solution.py:55
  32.8 1.4 scatter_custom_fusion
  34.2 12.6 %collective-permute-done.2 = bf16[512,2,128]{2,0,1:T(8,128)(2,1)S(1)} collective-permute-done((bf16[512,2,128]{2,0,1:T(8,128)(2,1)S(1)}, bf16[512,2,128]{2,0,1:T(8,128)(2,1)S(1)}, u32[]{:S(2)}, u32[]{:S(2)}) %collective-permute-start.2) | collective-permute-done | bytes 262176 | tf_op jit(solution)/shard_map/ppermute | solution.py:55
  47.2 1.3 copy.28
  48.6 1.3 copy.30
  50.1 9.8 %while.23 = (s32[]{:T(128)}, f32[2,512]{1,0:T(2,128)S(1)}, f32[2,512]{1,0:T(2,128)S(1)}, f32[2,512,128]{2,1,0:T(8,128)S(1)}, f32[2,512]{1,0:T(2,128)S(1)}, /*ind...) while((s32[]{:T(128)}, f32[2,512]{1,0:T(2,128)S(1)}, ...), condition=%wide.region_7.8_spmd.clone, body=%wide.region_0.7_spmd.clone.sunk | while | flops 410784768 | bytes 17183128 | solution.py:75
  51.3 4.6 %conditional.3 = ((f32[2,512]{1,0:T(2,128)S(1)}, f32[2,512]{1,0:T(2,128)S(1)}, f32[2,512,128]{2,1,0:T(8,128)S(1)}, f32[2,512]{1,0:T(2,128)S(1)}, f32[2,512]{1,0:T(2,128)S(1)}, /*index=5*/f32[2,512,128]{2,1,0:T(8,128)S(1)})) conditional(s32[]{:T(128)} %convert_element_type.87, (f32[2,512]{1,0:T(2,128)S(1)}, f32[2,512]{1,0:T(2,128)S(1)}, ...), branch_computations={%region_1.1_spmd, %region_2.6_spmd} | conditional | flops 410784768 | bytes 17180748 | solution.py:67
  60.4 2.1 bitcast_convert_fusion
  62.7 2.5 %gather_fusion = bf16[384,2048]{1,0:T(8,128)(2,1)S(1)} fusion(bf16[129,2048]{1,0:T(8,128)(2,1)S(1)} %concatenate.10, s32[1024]{0:T(1024)S(1)} %pad_clamp_fusion.1), kind=kCustom, calls=%fused_computation | custom fusion | bytes 3147264 | tf_op jit(solution)/shard_map/gather | solution.py:119
  65.1 33.0 %all_to_all.10 = bf16[4,96,2048]{2,1,0:T(8,128)(2,1)} all-to-all(bf16[4,96,2048]{2,1,0:T(8,128)(2,1)S(1)} %bitcast.62), channel_id=1, replica_groups=mesh['ep'=4,'tp'=8] {'ep'}, dimensions={0} | all-to-all | bytes 3145728 | tf_op jit(solution)/shard_map/all_to_all | solution.py:120
  98.1 5.7 %fusion.24 = f32[384,1024]{1,0:T(8,128)} fusion(bf16[384,2048]{1,0:T(8,128)(2,1)} %bitcast.64, bf16[1,2048,1024]{2,1,0:T(8,128)(2,1)} %all-gather.7.cloned.1.call-done), kind=kOutput, calls=%fused_computation.38 | convolution fusion | flops 1610612736 | bytes 7340032 | tf_op jit(solution)/shard_map/jrd,jdf->jrf/dot_general | solution.py:128
  103.8 39.4 %all-gather.11.cloned.1.call-done = bf16[1,2048,1024]{2,1,0:T(8,128)(2,1)} async-done(((bf16[1,2048,128]{2,1,0:T(8,128)(2,1)}), bf16[1,2048,1024]{2,1,0:T(8,128)(2,1)}) %all-gather.11.cloned.1.call-update) | async-done | bytes 4194320 | tf_op jit(solution)/shard_map/all_gather | solution.py:127
  143.2 47.5 %all-gather.9.cloned.1.call-done = bf16[1,2048,1024]{2,1,0:T(8,128)(2,1)} async-done(((bf16[1,2048,128]{2,1,0:T(8,128)(2,1)}), bf16[1,2048,1024]{2,1,0:T(8,128)(2,1)}) %all-gather.9.cloned.1.call-update) | async-done | bytes 4194320 | tf_op jit(solution)/shard_map/all_gather | solution.py:126
  190.7 8.6 %fusion.26 = bf16[384,2048]{1,0:T(8,128)(2,1)} fusion(bf16[1,2048,1024]{2,1,0:T(8,128)(2,1)} %all-gather.11.cloned.1.call-done, f32[384,1024]{1,0:T(8,128)} %fusion.24, bf16[384,2048]{1,0:T(8,128)(2,1)S(1)} %bitcast.65, bf16[1,2048,1024]{2,1,0:T(8,128)(2,1)} %all-gather.9.cloned.1.call-done), kind=kOutput, calls=%fused_computation.41 | convolution fusion | flops 3224371200 | bytes 13107200 | tf_op jit(solution)/shard_map/jrf,jdf->jrd/dot_general | solution.py:133
  199.3 3.8 %all-to-all-start.1 = ((bf16[4,96,2048]{2,1,0:T(8,128)(2,1)}), bf16[4,96,2048]{2,1,0:T(8,128)(2,1)S(1)}, u32[]{:S(2)}, u32[]{:S(2)}) async-start(bf16[4,96,2048]{2,1,0:T(8,128)(2,1)} %bitcast.66), calls=%async_computation.2 | async-start | bytes 3145728 | tf_op jit(solution)/shard_map/all_to_all | solution.py:140
  203.2 19.7 %all-to-all-done.1 = bf16[4,96,2048]{2,1,0:T(8,128)(2,1)S(1)} async-done(((bf16[4,96,2048]{2,1,0:T(8,128)(2,1)}), bf16[4,96,2048]{2,1,0:T(8,128)(2,1)S(1)}, u32[]{:S(2)}, u32[]{:S(2)}) %all-to-all-start.1) | async-done | bytes 1572896 | tf_op jit(solution)/shard_map/all_to_all | solution.py:140
  222.9 2.3 gather_fusion.1
  225.3 2.4 reshape.163
  227.7 3.9 %multiply_reduce_fusion = bf16[128,2048]{1,0:T(8,128)(2,1)} fusion(f32[128,2,2048]{2,1,0:T(2,128)S(1)} %reshape.163, f32[128,2]{1,0:T(8,128)S(1)} %copy.31), kind=kLoop, calls=%fused_computation.42 | loop fusion | flops 786432 | bytes 2622464 | tf_op jit(solution)/shard_map/reduce_sum | solution.py:145
  (109 shorter events, 12.6 us)
Async XLA Ops:
  7.2 53.2 %copy-start = (bf16[2,128,2048]{2,1,0:T(8,128)(2,1)S(1)}, bf16[2,128,2048]{2,1,0:T(8,128)(2,1)}, u32[]{:S(2)}) copy-start(bf16[2,128,2048]{2,1,0:T(8,128)(2,1)} %param.23) | copy-start | bytes 3145732
  7.2 4.0 %copy-start.1 = (bf16[512,2,128]{2,1,0:T(2,128)(2,1)S(1)}, bf16[512,2,128]{2,1,0:T(2,128)(2,1)}, u32[]{:S(2)}) copy-start(bf16[512,2,128]{2,1,0:T(2,128)(2,1)} %param.19) | copy-start | bytes 786436
  7.2 7.1 %copy-start.7 = (s32[128,2]{0,1:T(2,128)S(1)}, s32[128,2]{0,1:T(2,128)}, u32[]{:S(2)}) copy-start(s32[128,2]{0,1:T(2,128)} %param.26) | copy-start | bytes 3076
  7.2 7.4 %copy-start.2 = (bf16[128,2048]{1,0:T(8,128)(2,1)S(1)}, bf16[128,2048]{1,0:T(8,128)(2,1)}, u32[]{:S(2)}) copy-start(bf16[128,2048]{1,0:T(8,128)(2,1)} %param.24) | copy-start | bytes 1572868
  7.2 7.6 %copy-start.6 = (f32[2048]{0:T(1024)S(1)}, f32[2048]{0:T(1024)}, u32[]{:S(2)}) copy-start(f32[2048]{0:T(1024)} %param.25) | copy-start | bytes 24580
  7.2 41.4 %all-gather.5.cloned.1.call-start = ((), (), s32[]{:S(2)}) async-start(), calls=%async_computation.3 | async-start | bytes 1310720 | tf_op jit(solution)/shard_map/all_gather | solution.py:59
  9.1 23.5 %copy-start.5 = (bf16[512,2,128]{2,1,0:T(2,128)(2,1)S(1)}, bf16[512,2,128]{2,1,0:T(2,128)(2,1)}, u32[]{:S(2)}) copy-start(bf16[512,2,128]{2,1,0:T(2,128)(2,1)} %param.18) | copy-start | bytes 786436
  9.1 89.0 %all-gather.7.cloned.1.call-start = ((), (), s32[]{:S(2)}) async-start(), calls=%async_computation.5 | async-start | bytes 4718592 | tf_op jit(solution)/shard_map/all_gather | solution.py:125
  9.9 133.3 %all-gather.11.cloned.1.call-start = ((), (), s32[]{:S(2)}) async-start(), calls=%async_computation.7 | async-start | bytes 4718592 | tf_op jit(solution)/shard_map/all_gather | solution.py:127
  10.6 180.1 %all-gather.9.cloned.1.call-start = ((), (), s32[]{:S(2)}) async-start(), calls=%async_computation.6 | async-start | bytes 4718592 | tf_op jit(solution)/shard_map/all_gather | solution.py:126
  11.2 220.4 %reduce-scatter.2.cloned.1.call-start = ((), (), s32[]{:S(2)}) async-start(), calls=%async_computation.4 | async-start | bytes 2359296 | tf_op jit(solution)/shard_map/reduce_scatter | solution.py:86
  11.3 10.3 %collective-permute-start = (bf16[512,2,128]{2,0,1:T(8,128)(2,1)S(1)}, bf16[512,2,128]{2,0,1:T(8,128)(2,1)S(1)}, u32[]{:S(2)}, u32[]{:S(2)}) collective-permute-start(bf16[512,2,128]{2,0,1:T(8,128)(2,1)S(1)} %copy.24), channel_id=1, source_target_pairs={{0,8},{8,16},{16,24},{24,0},{1,9},{9,17},{17,25},{25,1},{2,10},{10... | collective-permute-start | bytes 786440 | tf_op jit(solution)/shard_map/ppermute | solution.py:55
  21.6 11.0 %collective-permute-start.1 = (bf16[512,2,128]{2,0,1:T(8,128)(2,1)S(1)}, bf16[512,2,128]{2,0,1:T(8,128)(2,1)S(1)}, u32[]{:S(2)}, u32[]{:S(2)}) collective-permute-start(bf16[512,2,128]{2,0,1:T(8,128)(2,1)S(1)} %collective-permute-done), channel_id=1, source_target_pairs={{0,8},{8,16},{16,24},{24,0},{1,9},{9,17},{17,25},{25,1},{2,10},{10... | collective-permute-start | bytes 786440 | tf_op jit(solution)/shard_map/ppermute | solution.py:55
  32.6 14.2 %collective-permute-start.2 = (bf16[512,2,128]{2,0,1:T(8,128)(2,1)S(1)}, bf16[512,2,128]{2,0,1:T(8,128)(2,1)S(1)}, u32[]{:S(2)}, u32[]{:S(2)}) collective-permute-start(bf16[512,2,128]{2,0,1:T(8,128)(2,1)S(1)} %collective-permute-done.1), channel_id=1, source_target_pairs={{0,8},{8,16},{16,24},{24,0},{1,9},{9,17},{17,25},{25,1},{2,10},{10... | collective-permute-start | bytes 786440 | tf_op jit(solution)/shard_map/ppermute | solution.py:55
  50.0 9.8 %copy-start.9 = (f32[2]{0:T(128)S(1)}, f32[2]{0:T(128)}, u32[]{:S(2)}) copy-start(f32[2]{0:T(128)} %param.21) | copy-start | bytes 28
  50.0 10.4 %copy-start.10 = (f32[128]{0:T(128)S(1)}, f32[128]{0:T(128)}, u32[]{:S(2)}) copy-start(f32[128]{0:T(128)} %param.22) | copy-start | bytes 1540
  60.4 2.2 copy-start.3
  98.1 92.6 %copy-start.4 = (bf16[4,96,2048]{2,1,0:T(8,128)(2,1)S(1)}, bf16[4,96,2048]{2,1,0:T(8,128)(2,1)}, u32[]{:S(2)}) copy-start(bf16[4,96,2048]{2,1,0:T(8,128)(2,1)} %all_to_all.10) | copy-start | bytes 4718596
  199.3 3.8 %copy-start.8 = (f32[128,2]{0,1:T(2,128)S(1)}, f32[128,2]{0,1:T(2,128)}, u32[]{:S(2)}) copy-start(f32[128,2]{0,1:T(2,128)} %param.28) | copy-start | bytes 3076
  199.3 3.8 %copy-start.11 = (f32[128]{0:T(128)S(1)}, f32[128]{0:T(128)}, u32[]{:S(2)}) copy-start(f32[128]{0:T(128)} %param.27) | copy-start | bytes 1540
  199.3 23.6 %all-to-all-start.1 = ((bf16[4,96,2048]{2,1,0:T(8,128)(2,1)}), bf16[4,96,2048]{2,1,0:T(8,128)(2,1)S(1)}, u32[]{:S(2)}, u32[]{:S(2)}) async-start(bf16[4,96,2048]{2,1,0:T(8,128)(2,1)} %bitcast.66), calls=%async_computation.2 | async-start | bytes 3145728 | tf_op jit(solution)/shard_map/all_to_all | solution.py:140
Sparse Core Ops, SparseCore 0:
  10.4 36.5 all-gather.4
  48.7 46.8 all-gather.6
  97.2 45.9 all-gather.10
  144.7 45.9 all-gather.8
  193.4 33.9 reduce-scatter.1
